TPU v7x, 512 devices: a whole 4x8x8 slice. The times are simulated.
512 devices in a mesh: sp: 64 (over z, y), tp: 8 (over x, core).
Axes of the slice: x: 4, y: 8, z: 8, core: 2. Of those that a mesh axis runs over, the one named last changes fastest.
Arguments:
- hidden_in: bfloat16 [24576, 2048], P('sp'), may hold values from -6 to 6
- drive: bfloat16 [24576, 1024], P('sp', 'tp'), may hold values from -24 to 24
- wide_poles: float32 [2, 32, 64], P(None, 'tp'), may hold values from -2 to 256, as said below
- narrow_poles: float32 [2, 32, 32], P(None, 'tp'), may hold values from -2 to 128, as said below
- log_step: float32 [32, 2], P('tp'), may hold values from -3.912 to -2.526
- forget: float32 [32, 2, 24576], P('tp', None, 'sp'), may hold values from 0 to 2
- wide_input: bfloat16 [2, 32, 64, 16], P(None, 'tp'), may hold values from -1 to 1
- narrow_input: bfloat16 [2, 32, 32, 16], P(None, 'tp'), may hold values from -1 to 1
- wide_output: bfloat16 [2, 32, 16, 64], P(None, 'tp'), may hold values from -0.5 to 0.5
- narrow_output: bfloat16 [2, 32, 16, 32], P(None, 'tp'), may hold values from -0.75 to 0.75
- skip: float32 [1024], P('tp'), may hold values from -4 to 4
- mix_gain: float32 [1024], P('tp'), may hold values from 0.1 to 1.9
- out_weight: bfloat16 [1024, 2048], P('tp'), may hold values from -0.1875 to 0.1875
- mlp_gain: float32 [2048], replicated, may hold values from 0.1 to 1.9
- up_weight: bfloat16 [2048, 8192], P('sp', 'tp'), may hold values from -0.125 to 0.125
- down_weight: bfloat16 [2048, 8192], P('sp', 'tp'), may hold values from -0.0625 to 0.0625
Outputs:
- hidden_out: bfloat16 [24576, 2048], P('sp')
Inputs may be any that keep to these rules, and one draw needn't show every extreme that they name: `wide_poles`: entry 0 holds real parts, each at most -1 / 24576; entry 1 holds imaginary parts. `narrow_poles`: entry 0 holds real parts, each at most -1 / 24576; entry 1 holds imaginary parts.
All inputs are finite; a program needn't handle non-finite values.
Results may differ from a plain program's by a relative error of at most 0.02.
Values may be sent and summed in bfloat16 or wider, within the bound.
No kernel may reach another device: no remote copies, remote signals or barrier semaphores. Data moves between devices by JAX's collectives and lax.ppermute only.
A program may use at most 64 MiB of HBM per device.

v0:
```python
import jax
import jax.numpy as jnp
from jax import lax
from jax.sharding import PartitionSpec as P

epsilon = 1e-06


def copy_for_each(value, axis):
    count = lax.axis_size(axis)
    return lax.all_to_all(
        jnp.broadcast_to(value[None], (count, *value.shape)), axis, 0, 0, tiled=True
    )


def gathered_once(value, axis):
    leaves = jax.tree.leaves(value)
    turns = sorted(range(len(leaves)), key=lambda k: -leaves[k].size)
    width = (1, *leaves[turns[0]].shape)[-1]
    lines = [
        jnp.pad(leaves[k].reshape(-1), (0, -leaves[k].size % width)).reshape(-1, width)
        for k in turns
    ]
    both, at, found = (copy_for_each(jnp.concatenate(lines), axis), 0, {})
    for k, line in zip(turns, lines):
        slab = both[:, at : at + len(line)].reshape(len(both), -1)
        found[k] = slab[:, : leaves[k].size].reshape(-1, *leaves[k].shape)
        at += len(line)
    numbers = iter(range(len(leaves)))
    return jax.tree.map(lambda _: found[next(numbers)], value)


def joined_by_halves(pieces, combine):
    while len(jax.tree.leaves(pieces)[0]) > 1:
        pieces = jax.vmap(combine)(
            *(jax.tree.map(lambda part: part[side::2], pieces) for side in (0, 1))
        )
    return jax.tree.map(lambda part: part[0], pieces)


def carried_in(value, axis, combine, identity):
    count, here = (lax.axis_size(axis), lax.axis_index(axis))
    passed = jnp.arange(count) < here

    def kept(part, zero, own):
        part = jnp.where(
            passed.reshape(-1, *(1 for _ in own.shape)), part, jnp.asarray(zero, own.dtype)
        )
        return part

    pieces = gathered_once(value, axis)
    return joined_by_halves(jax.tree.map(kept, pieces, identity, value), combine)


def of_everyone(value, axis):
    return copy_for_each(value, axis).sum(axis=0)


def split_up(value, dim, count):
    dims = value.shape
    pieces = value.reshape(*dims[:dim], count, dims[dim] // count, *dims[dim + 1 :])
    return jnp.moveaxis(pieces, dim, 0)


def sum_at_owner(value, axis, dim):
    count = lax.axis_size(axis)
    pieces = lax.all_to_all(split_up(value, dim, count), axis, 0, 0, tiled=True)
    return jnp.sum(pieces.astype(jnp.float32), axis=0)


def in_order(pieces, dim):
    pieces = jnp.moveaxis(pieces, 0, dim)
    dims = pieces.shape
    return pieces.reshape(*dims[:dim], dims[dim] * dims[dim + 1], *dims[dim + 2 :])


def collect(value, axis, dim):
    pieces = copy_for_each(value, axis)
    return in_order(pieces, dim)


def combine(earlier, later):
    return (
        later[0] * earlier[0] - later[1] * earlier[1],
        later[0] * earlier[1] + later[1] * earlier[0],
        later[0] * earlier[2] - later[1] * earlier[3] + later[2],
        later[0] * earlier[3] + later[1] * earlier[2] + later[3],
    )


def combine_both(earlier, later):
    return combine(earlier[:4], later[:4]) + combine(earlier[4:], later[4:])


def discretize(pole_pair, log_rate):
    step_size = jnp.exp(log_rate)[:, None]
    growth = pole_pair[0] * step_size
    angle = pole_pair[1] * step_size
    rise_real = jnp.expm1(growth) * jnp.cos(angle) - 2.0 * jnp.sin(0.5 * angle) ** 2
    rise_imag = jnp.exp(growth) * jnp.sin(angle)
    denominator = pole_pair[0] ** 2 + pole_pair[1] ** 2
    coef_real = (rise_real * pole_pair[0] + rise_imag * pole_pair[1]) / denominator
    coef_imag = (rise_imag * pole_pair[0] - rise_real * pole_pair[1]) / denominator
    return (growth.reshape(-1), angle.reshape(-1), coef_real.reshape(-1), coef_imag.reshape(-1))


def kind_states(drive, forget_kind, pole_pair, log_rate, in_weight, kind_index):
    pair_count, state_len = (pole_pair.shape[1], pole_pair.shape[2])
    growth, angle, coef_real, coef_imag = discretize(pole_pair, log_rate)
    diagonal = jnp.eye(pair_count, dtype=jnp.bfloat16)
    select = (jnp.arange(2) == kind_index).astype(jnp.bfloat16)
    in_block = jnp.einsum("pq,k,rpsh->pkhrqs", diagonal, select, in_weight).reshape(
        pair_count * 2 * in_weight.shape[3], 2 * pair_count * state_len
    )
    pushed = jnp.dot(drive, in_block, preferred_element_type=jnp.float32)
    width = pair_count * state_len
    drive_real = pushed[:, :width]
    drive_imag = pushed[:, width:]
    push_real = coef_real * drive_real - coef_imag * drive_imag
    push_imag = coef_real * drive_imag + coef_imag * drive_real
    spread = jnp.repeat(jnp.eye(pair_count, dtype=jnp.float32), state_len, axis=1)
    decay_rows = lax.dot_general(forget_kind, spread, (((0,), (0,)), ((), ())))
    spike_magnitude = jnp.exp(growth[None] - decay_rows)
    return lax.associative_scan(
        combine,
        (
            spike_magnitude * jnp.cos(angle)[None],
            spike_magnitude * jnp.sin(angle)[None],
            push_real,
            push_imag,
        ),
        axis=0,
    )


def read_out(state_real, state_imag, out_kind, kind_index):
    pair_count, group_len, state_len = (out_kind.shape[1], out_kind.shape[2], out_kind.shape[3])
    diagonal = jnp.eye(pair_count, dtype=jnp.float32)
    select = (jnp.arange(2) == kind_index).astype(jnp.float32)
    total_columns = pair_count * 2 * group_len

    def out_block(part_index):
        return jnp.einsum(
            "qp,k,pgs->qspkg", diagonal, select, out_kind[part_index].astype(jnp.float32)
        ).reshape(pair_count * state_len, total_columns)

    first = jnp.dot(state_real, out_block(0))
    second = jnp.dot(state_imag, out_block(1))
    return first - second


def row_norm(rows_in, gain):
    values = rows_in.astype(jnp.float32)
    return (
        values * lax.rsqrt(jnp.mean(values * values, axis=1, keepdims=True) + epsilon) * gain
    ).astype(jnp.bfloat16)


def local(
    hidden_in,
    drive,
    wide_poles,
    narrow_poles,
    log_step,
    forget,
    wide_input,
    narrow_input,
    wide_output,
    narrow_output,
    skip,
    mix_gain,
    out_weight,
    mlp_gain,
    up_weight,
    down_weight,
):
    row_count = drive.shape[0]
    up_whole, down_whole = (
        lax.all_gather(up_weight, "sp", axis=0, tiled=True),
        lax.all_gather(down_weight, "sp", axis=0, tiled=True),
    )
    kinds = ((wide_poles, wide_input, wide_output), (narrow_poles, narrow_input, narrow_output))
    scanned = [
        kind_states(
            drive,
            forget[:, kind_index, :],
            kinds[kind_index][0],
            log_step[:, kind_index],
            kinds[kind_index][1],
            kind_index,
        )
        for kind_index in range(2)
    ]
    ends = tuple((member[-1] for member in scanned[0])) + tuple(
        (member[-1] for member in scanned[1])
    )
    identity = tuple(
        (
            jnp.ones_like(member) if position % 4 == 0 else jnp.zeros_like(member)
            for position, member in enumerate(ends)
        )
    )
    entering = carried_in(ends, "sp", combine_both, identity)
    response = skip[None, :] * drive.astype(jnp.float32)
    for kind_index in range(2):
        cum_real, cum_imag, local_real, local_imag = scanned[kind_index]
        start_real = entering[4 * kind_index + 2][None]
        start_imag = entering[4 * kind_index + 3][None]
        state_real = local_real + cum_real * start_real - cum_imag * start_imag
        state_imag = local_imag + cum_real * start_imag + cum_imag * start_real
        response = response + read_out(state_real, state_imag, kinds[kind_index][2], kind_index)
    active = jax.nn.gelu(response, approximate=False)
    power = of_everyone(jnp.sum(active * active, axis=1), "tp")
    channel_total = drive.shape[1] * lax.axis_size("tp")
    mixed = (active * lax.rsqrt(power / channel_total + epsilon)[:, None] * mix_gain).astype(
        jnp.bfloat16
    )
    share = row_count // lax.axis_size("tp")
    proj_sum = sum_at_owner(
        jnp.dot(mixed, out_weight, preferred_element_type=jnp.float32).astype(jnp.bfloat16), "tp", 0
    )
    own_rows = lax.dynamic_slice_in_dim(hidden_in, lax.axis_index("tp") * share, share, 0)
    carried_rows = (own_rows.astype(jnp.float32) + proj_sum).astype(jnp.bfloat16)
    gathered = collect(row_norm(carried_rows, mlp_gain), "tp", 0)
    pre_act = jnp.dot(gathered, up_whole, preferred_element_type=jnp.float32)
    squared = jnp.square(jax.nn.relu(pre_act)).astype(jnp.bfloat16)
    partial_value = lax.dot_general(
        squared, down_whole, (((1,), (1,)), ((), ())), preferred_element_type=jnp.float32
    )
    mixer_sum = sum_at_owner(partial_value.astype(jnp.bfloat16), "tp", 0)
    completed_result = (carried_rows.astype(jnp.float32) + mixer_sum).astype(jnp.bfloat16)
    return collect(completed_result, "tp", 0)


def solution(mesh):
    return jax.shard_map(
        local,
        mesh=mesh,
        in_specs=(
            P("sp", None),
            P("sp", "tp"),
            P(None, "tp", None),
            P(None, "tp", None),
            P("tp", None),
            P("tp", None, "sp"),
            P(None, "tp", None, None),
            P(None, "tp", None, None),
            P(None, "tp", None, None),
            P(None, "tp", None, None),
            P("tp"),
            P("tp"),
            P("tp", None),
            P(),
            P("sp", "tp"),
            P("sp", "tp"),
        ),
        out_specs=P("sp", None),
        check_vma=False,
    )
```

profile of v0, /device:TPU:1, one launch (start us, length us, event | category | flops | bytes accessed | tf_op | source)
XLA Modules:
  0.0 431.1 jit_solution(17403516793321845758)
XLA Ops:
  55.4 1.5 multiply_subtract_fusion.3
  62.2 1.9 add_add_fusion.5
  68.0 1.5 slice.1383
  69.5 1.5 slice.1392
  71.0 1.7 multiply_subtract_fusion.11
  73.9 1.4 slice.1389
  75.3 1.4 slice.1396
  76.7 1.4 slice.1391
  78.1 1.4 slice.1397
  79.5 1.4 slice.1393
  80.9 1.4 slice.1402
  82.3 1.5 add_add_fusion.14
  83.8 1.3 slice.1400
  85.1 1.3 slice.1404
  87.7 1.3 slice.1401
  89.0 1.3 slice.1407
  90.4 1.3 slice.1403
  91.7 1.3 slice.1412
  93.0 1.5 multiply_subtract_fusion.20
  94.5 1.3 slice.1410
  95.8 1.3 slice.1414
  97.2 1.3 slice.1409
  105.0 1.4 add_add_fusion.26
  132.9 1.3 slice.1449
  134.2 1.3 slice.1453
  135.6 1.3 slice.1457
  139.5 1.4 slice.1388
  140.9 1.4 slice.1455
  142.9 1.4 slice.1463
  147.4 1.5 slice.1469
  195.0 1.6 pad.434
  196.7 1.6 pad.433
  203.7 17.3 %all-to-all-start = ((f32[64,8,256]{2,1,0:T(8,128)}), f32[64,8,256]{2,1,0:T(8,128)S(1)}, u32[]{:S(2)}, u32[]{:S(2)}) async-start(f32[64,8,256]{2,1,0:T(8,128)} %broadcast_in_dim.98), calls=%async_computation | async-start | bytes 1048576 | tf_op jit(solution)/shard_map/all_to_all | solution.py:11
  223.5 1.6 reshape.360
  226.7 1.7 reshape.352
  228.4 1.7 reshape.354
  230.8 7.7 %all-to-all-done = f32[64,8,256]{2,1,0:T(8,128)S(1)} async-done(((f32[64,8,256]{2,1,0:T(8,128)}), f32[64,8,256]{2,1,0:T(8,128)S(1)}, u32[]{:S(2)}, u32[]{:S(2)}) %all-to-all-start) | async-done | bytes 524320 | tf_op jit(solution)/shard_map/all_to_all | solution.py:11
  250.3 1.5 slice.1680
  251.8 1.4 slice.1681
  253.2 1.4 slice.1700
  254.7 1.4 slice.1703
  256.1 1.4 slice.1702
  257.6 1.5 slice.1705
  259.0 1.5 multiply_subtract_fusion.12
  260.6 1.4 slice.1682
  261.9 1.4 slice.1683
  263.3 1.4 slice.1684
  264.6 1.4 slice.1685
  266.0 1.4 slice.1704
  267.4 1.4 slice.1707
  268.7 1.4 slice.1706
  270.1 1.4 slice.1709
  271.4 1.5 multiply_subtract_fusion.18
  275.5 1.3 slice.1688
  282.0 1.4 multiply_subtract_fusion.24
  296.9 1.5 fusion.31
  301.3 11.9 %all_to_all.31 = f32[8,1,384]{2,1,0:T(1,128)S(1)} all-to-all(f32[8,1,384]{2,1,0:T(1,128)S(1)} %broadcast_in_dim.104), channel_id=1, replica_groups=mesh['sp'=64,'tp'=8] {'tp'}, dimensions={0} | all-to-all | bytes 24576 | tf_op jit(solution)/shard_map/all_to_all | solution.py:11
  313.3 1.8 convolution_convert_fusion.1
  315.1 4.2 all-to-all-start.2
  319.3 20.6 %all-to-all-done.2 = bf16[8,48,2048]{2,1,0:T(8,128)(2,1)S(1)} async-done(((bf16[8,48,2048]{2,1,0:T(8,128)(2,1)}), bf16[8,48,2048]{2,1,0:T(8,128)(2,1)S(1)}, u32[]{:S(2)}, u32[]{:S(2)}) %all-to-all-start.2) | async-done | bytes 1572896 | tf_op jit(solution)/shard_map/all_to_all | solution.py:67
  341.6 23.9 %all_to_all.32 = bf16[8,48,2048]{2,1,0:T(8,128)(2,1)S(1)} all-to-all(bf16[8,48,2048]{2,1,0:T(8,128)(2,1)S(1)} %broadcast_in_dim.105), channel_id=1, replica_groups=mesh['sp'=64,'tp'=8] {'tp'}, dimensions={0} | all-to-all | bytes 3145728 | tf_op jit(solution)/shard_map/all_to_all | solution.py:11
  365.5 8.0 %convolution_convert_fusion = bf16[384,2048]{1,0:T(8,128)(2,1)} fusion(bf16[2048,1024]{1,0:T(8,128)(2,1)} %all-gather.5.cloned.1.call-done, bf16[384,2048]{1,0:T(8,128)(2,1)S(1)} %bitcast.131, bf16[2048,1024]{1,0:T(8,128)(2,1)} %all-gather.3.cloned.1.call-done), kind=kOutput, calls=%fused_computation.2 | convolution fusion | flops 3223191552 | bytes 11534336 | tf_op jit(solution)/shard_map/dot_general | solution.py:227
  373.6 25.1 %all_to_all.33 = bf16[8,48,2048]{2,1,0:T(8,128)(2,1)S(1)} all-to-all(bf16[8,48,2048]{2,1,0:T(8,128)(2,1)} %bitcast.132), channel_id=1, replica_groups=mesh['sp'=64,'tp'=8] {'tp'}, dimensions={0} | all-to-all | bytes 3145728 | tf_op jit(solution)/shard_map/all_to_all | solution.py:67
  399.1 24.0 %all_to_all.34 = bf16[8,48,2048]{2,1,0:T(8,128)(2,1)S(1)} all-to-all(bf16[8,48,2048]{2,1,0:T(8,128)(2,1)S(1)} %broadcast_in_dim.106), channel_id=1, replica_groups=mesh['sp'=64,'tp'=8] {'tp'}, dimensions={0} | all-to-all | bytes 3145728 | tf_op jit(solution)/shard_map/all_to_all | solution.py:11
  (916 shorter events, 191.5 us)
Async XLA Ops:
  6.5 306.8 %copy-start = (bf16[128,2048]{1,0:T(8,128)(2,1)S(1)}, bf16[128,2048]{1,0:T(8,128)(2,1)}, u32[]{:S(2)}) copy-start(bf16[128,2048]{1,0:T(8,128)(2,1)} %param.28) | copy-start | bytes 1572868
  6.5 5.5 %copy-start.3 = (bf16[384,128]{1,0:T(8,128)(2,1)S(1)}, bf16[384,128]{1,0:T(8,128)(2,1)}, u32[]{:S(2)}) copy-start(bf16[384,128]{1,0:T(8,128)(2,1)} %param.17) | copy-start | bytes 294916
  6.5 359.0 %all-gather.3.cloned.1.call-start = ((), (), s32[]{:S(2)}) async-start(), calls=%async_computation.6 | async-start | bytes 4259840 | tf_op jit(solution)/shard_map/all_gather | solution.py:179
  12.6 35.8 %copy-start.117 = (f32[2,4,64]{2,1,0:T(4,128)S(1)}, f32[2,4,64]{2,1,0:T(4,128)}, u32[]{:S(2)}) copy-start(f32[2,4,64]{2,1,0:T(4,128)} %param.18) | copy-start | bytes 6148
  39.5 12.2 %copy-start.63 = (bf16[2,4,64,16]{2,3,1,0:T(8,128)(2,1)S(1)}, bf16[2,4,64,16]{2,3,1,0:T(8,128)(2,1)}, u32[]{:S(2)}) copy-start(bf16[2,4,64,16]{2,3,1,0:T(8,128)(2,1)} %param.22) | copy-start | bytes 49156
  64.2 82.0 %copy-start.16 = (f32[96,256]{1,0:T(8,128)}, f32[96,256]{1,0:T(8,128)S(1)}, u32[]{:S(2)}) copy-start(f32[96,256]{1,0:T(8,128)S(1)} %get-tuple-element.86) | copy-start | bytes 294916
  156.2 29.5 %copy-start.135 = (f32[1,128]{1,0:T(1,128)S(1)}, f32[1,128]{1,0:T(1,128)}, u32[]{:S(2)}) copy-start(f32[1,128]{1,0:T(1,128)} %slice.1893) | copy-start | bytes 1540
  156.2 29.6 %copy-start.34 = (f32[47,128]{1,0:T(8,128)S(1)}, f32[47,128]{1,0:T(8,128)}, u32[]{:S(2)}) copy-start(f32[47,128]{1,0:T(8,128)} %slice.1531) | copy-start | bytes 72196
  156.2 29.6 %copy-start.35 = (f32[47,128]{1,0:T(8,128)S(1)}, f32[47,128]{1,0:T(8,128)}, u32[]{:S(2)}) copy-start(f32[47,128]{1,0:T(8,128)} %slice.1582) | copy-start | bytes 72196
  156.2 29.6 %copy-start.51 = (f32[47,128]{1,0:T(8,128)S(1)}, f32[47,128]{1,0:T(8,128)}, u32[]{:S(2)}) copy-start(f32[47,128]{1,0:T(8,128)} %slice.1661) | copy-start | bytes 72196
  156.2 29.6 %copy-start.52 = (f32[47,128]{1,0:T(8,128)S(1)}, f32[47,128]{1,0:T(8,128)}, u32[]{:S(2)}) copy-start(f32[47,128]{1,0:T(8,128)} %slice.1664) | copy-start | bytes 72196
  156.2 29.7 %copy-start.132 = (f32[1,128]{1,0:T(1,128)S(1)}, f32[1,128]{1,0:T(1,128)}, u32[]{:S(2)}) copy-start(f32[1,128]{1,0:T(1,128)} %slice.1951) | copy-start | bytes 1540
  156.2 29.7 %copy-start.131 = (f32[1,128]{1,0:T(1,128)S(1)}, f32[1,128]{1,0:T(1,128)}, u32[]{:S(2)}) copy-start(f32[1,128]{1,0:T(1,128)} %slice.1930) | copy-start | bytes 1540
  156.2 29.8 %copy-start.134 = (f32[1,128]{1,0:T(1,128)S(1)}, f32[1,128]{1,0:T(1,128)}, u32[]{:S(2)}) copy-start(f32[1,128]{1,0:T(1,128)} %slice.1913) | copy-start | bytes 1540
  156.2 29.8 %copy-start.133 = (f32[1,128]{1,0:T(1,128)S(1)}, f32[1,128]{1,0:T(1,128)}, u32[]{:S(2)}) copy-start(f32[1,128]{1,0:T(1,128)} %slice.1892) | copy-start | bytes 1540
  179.4 6.8 %copy-start.18 = (f32[95,128]{1,0:T(8,128)S(1)}, f32[95,128]{1,0:T(8,128)}, u32[]{:S(2)}) copy-start(f32[95,128]{1,0:T(8,128)} %slice.1525) | copy-start | bytes 145924
  179.4 6.8 %copy-start.19 = (f32[95,128]{1,0:T(8,128)S(1)}, f32[95,128]{1,0:T(8,128)}, u32[]{:S(2)}) copy-start(f32[95,128]{1,0:T(8,128)} %slice.1586) | copy-start | bytes 145924
  182.1 4.2 copy-start.40
  182.1 4.2 copy-start.41
  187.5 4.6 %copy-start.64 = (f32[2,256]{1,0:T(2,128)S(1)}, f32[2,256]{1,0:T(2,128)}, u32[]{:S(2)}) copy-start(f32[2,256]{1,0:T(2,128)} %slice.1418) | copy-start | bytes 6148
  187.5 4.6 %copy-start.66 = (f32[2,256]{1,0:T(2,128)S(1)}, f32[2,256]{1,0:T(2,128)}, u32[]{:S(2)}) copy-start(f32[2,256]{1,0:T(2,128)} %slice.1438) | copy-start | bytes 6148
  187.5 4.6 %copy-start.83 = (f32[2,256]{1,0:T(2,128)S(1)}, f32[2,256]{1,0:T(2,128)}, u32[]{:S(2)}) copy-start(f32[2,256]{1,0:T(2,128)} %slice.1441) | copy-start | bytes 6148
  187.5 4.6 %copy-start.84 = (f32[2,256]{1,0:T(2,128)S(1)}, f32[2,256]{1,0:T(2,128)}, u32[]{:S(2)}) copy-start(f32[2,256]{1,0:T(2,128)} %slice.1445) | copy-start | bytes 6148
  187.5 4.6 %copy-start.112 = (f32[1,256]{1,0:T(1,128)S(1)}, f32[1,256]{1,0:T(1,128)}, u32[]{:S(2)}) copy-start(f32[1,256]{1,0:T(1,128)} %slice.1809) | copy-start | bytes 3076
  187.5 4.7 %copy-start.111 = (f32[1,256]{1,0:T(1,128)S(1)}, f32[1,256]{1,0:T(1,128)}, u32[]{:S(2)}) copy-start(f32[1,256]{1,0:T(1,128)} %slice.1792) | copy-start | bytes 3076
  187.5 4.7 %copy-start.53 = (f32[5,256]{1,0:T(8,128)S(1)}, f32[5,256]{1,0:T(8,128)}, u32[]{:S(2)}) copy-start(f32[5,256]{1,0:T(8,128)} %slice.1408) | copy-start | bytes 15364
  187.5 4.7 %copy-start.55 = (f32[5,256]{1,0:T(8,128)S(1)}, f32[5,256]{1,0:T(8,128)}, u32[]{:S(2)}) copy-start(f32[5,256]{1,0:T(8,128)} %slice.1443) | copy-start | bytes 15364
  187.5 4.7 %copy-start.61 = (f32[5,256]{1,0:T(8,128)S(1)}, f32[5,256]{1,0:T(8,128)}, u32[]{:S(2)}) copy-start(f32[5,256]{1,0:T(8,128)} %slice.1447) | copy-start | bytes 15364
  187.6 4.7 %copy-start.62 = (f32[5,256]{1,0:T(8,128)S(1)}, f32[5,256]{1,0:T(8,128)}, u32[]{:S(2)}) copy-start(f32[5,256]{1,0:T(8,128)} %slice.1451) | copy-start | bytes 15364
  187.6 4.7 %copy-start.110 = (f32[1,256]{1,0:T(1,128)S(1)}, f32[1,256]{1,0:T(1,128)}, u32[]{:S(2)}) copy-start(f32[1,256]{1,0:T(1,128)} %slice.1814) | copy-start | bytes 3076
  187.6 4.8 %copy-start.109 = (f32[1,256]{1,0:T(1,128)S(1)}, f32[1,256]{1,0:T(1,128)}, u32[]{:S(2)}) copy-start(f32[1,256]{1,0:T(1,128)} %slice.1791) | copy-start | bytes 3076
  187.6 4.8 %copy-start.44 = (f32[11,256]{1,0:T(8,128)S(1)}, f32[11,256]{1,0:T(8,128)}, u32[]{:S(2)}) copy-start(f32[11,256]{1,0:T(8,128)} %slice.1398) | copy-start | bytes 33796
  187.6 4.8 %copy-start.46 = (f32[11,256]{1,0:T(8,128)S(1)}, f32[11,256]{1,0:T(8,128)}, u32[]{:S(2)}) copy-start(f32[11,256]{1,0:T(8,128)} %slice.1449) | copy-start | bytes 33796
  187.6 4.8 %copy-start.57 = (f32[11,256]{1,0:T(8,128)S(1)}, f32[11,256]{1,0:T(8,128)}, u32[]{:S(2)}) copy-start(f32[11,256]{1,0:T(8,128)} %slice.1453) | copy-start | bytes 33796
  187.7 4.8 %copy-start.58 = (f32[11,256]{1,0:T(8,128)S(1)}, f32[11,256]{1,0:T(8,128)}, u32[]{:S(2)}) copy-start(f32[11,256]{1,0:T(8,128)} %slice.1457) | copy-start | bytes 33796
  188.4 4.1 copy-start.108
  188.4 4.2 copy-start.107
  188.4 4.2 copy-start.30
  188.5 4.2 copy-start.32
  188.5 4.2 copy-start.49
  188.5 4.2 copy-start.50
  188.5 4.3 copy-start.106
  194.9 3.8 copy-start.45
  194.9 3.8 copy-start.47
  194.9 3.9 copy-start.100
  194.9 3.9 copy-start.99
  194.9 3.9 copy-start.31
  195.0 3.9 copy-start.33
  195.0 4.0 copy-start.98
  195.0 4.0 copy-start.97
  201.9 19.9 %copy-start.69 = (f32[4,4]{0,1:T(4,128)S(1)}, f32[4,4]{0,1:T(4,128)}, u32[]{:S(2)}) copy-start(f32[4,4]{0,1:T(4,128)} %copy-done.68) | copy-start | bytes 196
  201.9 20.7 %copy-start.59 = (bf16[2,4,16,32]{3,2,1,0:T(8,128)(2,1)S(1)}, bf16[2,4,16,32]{3,2,1,0:T(8,128)(2,1)}, u32[]{:S(2)}) copy-start(bf16[2,4,16,32]{3,2,1,0:T(8,128)(2,1)} %param.25) | copy-start | bytes 24580
  203.7 34.8 %all-to-all-start = ((f32[64,8,256]{2,1,0:T(8,128)}), f32[64,8,256]{2,1,0:T(8,128)S(1)}, u32[]{:S(2)}, u32[]{:S(2)}) async-start(f32[64,8,256]{2,1,0:T(8,128)} %broadcast_in_dim.98), calls=%async_computation | async-start | bytes 1048576 | tf_op jit(solution)/shard_map/all_to_all | solution.py:11
  221.0 144.5 %all-gather.5.cloned.1.call-start = ((), (), s32[]{:S(2)}) async-start(), calls=%async_computation.7 | async-start | bytes 4259840 | tf_op jit(solution)/shard_map/all_gather | solution.py:180
  239.5 8.8 %copy-start.27 = (f32[64,1,256]{2,1,0:T(1,128)S(1)}, f32[64,1,256]{2,1,0:T(1,128)}, u32[]{:S(2)}) copy-start(f32[64,1,256]{2,1,0:T(1,128)} %get-tuple-element.47) | copy-start | bytes 196612
  239.5 8.8 %copy-start.28 = (f32[64,1,256]{2,1,0:T(1,128)S(1)}, f32[64,1,256]{2,1,0:T(1,128)}, u32[]{:S(2)}) copy-start(f32[64,1,256]{2,1,0:T(1,128)} %get-tuple-element.48) | copy-start | bytes 196612
  239.5 8.8 %copy-start.29 = (f32[64,1,256]{2,1,0:T(1,128)S(1)}, f32[64,1,256]{2,1,0:T(1,128)}, u32[]{:S(2)}) copy-start(f32[64,1,256]{2,1,0:T(1,128)} %get-tuple-element.49) | copy-start | bytes 196612
  240.8 56.1 %copy-start.5 = (f32[384,128]{1,0:T(8,128)S(1)}, f32[384,128]{1,0:T(8,128)}, u32[]{:S(2)}) copy-start(f32[384,128]{1,0:T(8,128)} %copy-done.4) | copy-start | bytes 589828
  250.3 48.2 %copy-start.1 = (f32[384,256]{1,0:T(8,128)S(1)}, f32[384,256]{1,0:T(8,128)}, u32[]{:S(2)}) copy-start(f32[384,256]{1,0:T(8,128)} %pad.434) | copy-start | bytes 1179652
  250.3 48.2 %copy-start.26 = (bf16[256,128]{0,1:T(8,128)(2,1)S(1)}, bf16[256,128]{0,1:T(8,128)(2,1)}, u32[]{:S(2)}) copy-start(bf16[256,128]{0,1:T(8,128)(2,1)} %reshape.352) | copy-start | bytes 196612
  294.7 3.8 copy-start.2
  300.7 12.6 %copy-start.122 = (f32[128]{0:T(128)S(1)}, f32[128]{0:T(128)}, u32[]{:S(2)}) copy-start(f32[128]{0:T(128)} %param.27) | copy-start | bytes 1540
  315.1 24.8 %all-to-all-start.2 = ((bf16[8,48,2048]{2,1,0:T(8,128)(2,1)}), bf16[8,48,2048]{2,1,0:T(8,128)(2,1)S(1)}, u32[]{:S(2)}, u32[]{:S(2)}) async-start(bf16[8,48,2048]{2,1,0:T(8,128)(2,1)} %bitcast.42), calls=%async_computation.2 | async-start | bytes 3145728 | tf_op jit(solution)/shard_map/all_to_all | solution.py:67
  319.3 22.0 %copy-start.82 = (f32[2048]{0:T(1024)S(1)}, f32[2048]{0:T(1024)}, u32[]{:S(2)}) copy-start(f32[2048]{0:T(1024)} %param.29) | copy-start | bytes 24580
  (77 other events, 166.3 us)
Sparse Core Ops, SparseCore 0:
  10.4 88.1 all-gather.2
  224.9 83.7 all-gather.4
where the time goes:
time: 438 us; the launch traced here: 431 us
  local copies, waits for them, and re-layouts  221 us (50%)
  blocking collectives  85 us (19%)
  other arithmetic  42.6 us (10%)
  waiting for transfers between devices  29.7 us (7%)
  starting transfers between devices  21.6 us (5%)
  between operations  17.3 us (4%)
  matrix products  13.5 us (3%)
    slice x224, local copies, waits for them, and re-layouts, kind_states(): lax.associative_scan(combine, (spike_magnitude * jnp.cos(angle)[None], sp...  146 us
    all_to_all x3, blocking collectives, copy_for_each(): lax.all_to_all(jnp.broadcast_to(value[None], (count, *value.shape)), axis...  59.9 us
    slice x80, local copies, waits for them, and re-layouts, joined_by_halves(): part[side::2]  47.9 us
    all_to_all x1, blocking collectives, sum_at_owner(): pieces = lax.all_to_all(split_up(value, dim, count), axis, 0, 0, tiled=True)  25.1 us
    all_to_all x1, waiting for transfers between devices, sum_at_owner(): pieces = lax.all_to_all(split_up(value, dim, count), axis, 0, 0, tiled=True)  20.6 us
    all_to_all x1, starting transfers between devices, copy_for_each(): lax.all_to_all(jnp.broadcast_to(value[None], (count, *value.shape)), axis...  17.3 us
    sub x13, other arithmetic, combine(): later[0] * earlier[0] - later[1] * earlier[1]  10.6 us
    concatenate x64, other arithmetic, kind_states(): lax.associative_scan(combine, (spike_magnitude * jnp.cos(angle)[None], sp...  10.2 us
  transfers between devices with their start and end apart: 4, of which 2 were waited for; matrix products, arithmetic and copies ran while one was open for 61% of the time, Pallas kernels for 0%

commit v1 on v0

v1 whole, which is shorter than its diff:
```python
import functools

import jax
import jax.numpy as jnp
from jax import lax
from jax.experimental import pallas as pl
from jax.experimental.pallas import tpu as pltpu
from jax.sharding import PartitionSpec as P

epsilon = 1e-06
bf16, f32 = jnp.bfloat16, jnp.float32
WHOLE = pl.BlockSpec(memory_space=pltpu.VMEM)
SCALARS = pl.BlockSpec(memory_space=pltpu.SMEM)
CHUNKS = 8
LANES = 128
GAIN_ROWS = 16


def copy_for_each(value, axis, groups=None):
    count = len(groups[0]) if groups else lax.axis_size(axis)
    return lax.all_to_all(
        jnp.broadcast_to(value[None], (count, *value.shape)),
        axis,
        0,
        0,
        tiled=True,
        axis_index_groups=groups,
    )


def discretize(pole_pair, log_rate):
    step_size = jnp.exp(log_rate)[:, None]
    growth = pole_pair[0] * step_size
    angle = pole_pair[1] * step_size
    rise_real = jnp.expm1(growth) * jnp.cos(angle) - 2.0 * jnp.sin(0.5 * angle) ** 2
    rise_imag = jnp.exp(growth) * jnp.sin(angle)
    denominator = pole_pair[0] ** 2 + pole_pair[1] ** 2
    coef_real = (rise_real * pole_pair[0] + rise_imag * pole_pair[1]) / denominator
    coef_imag = (rise_imag * pole_pair[0] - rise_real * pole_pair[1]) / denominator
    terms = (growth, jnp.cos(angle), jnp.sin(angle), coef_real, coef_imag)
    return jnp.stack([term.reshape(-1) for term in terms])


def times(a, b):
    return a[0] * b[0] - a[1] * b[1], a[0] * b[1] + a[1] * b[0]


def power_of(phase, exponent):
    result = None
    while exponent:
        if exponent & 1:
            result = phase if result is None else times(result, phase)
        exponent >>= 1
        if exponent:
            phase = times(phase, phase)
    return result


def owners(rows, states, pairs, group, wide):
    row = lax.broadcasted_iota(jnp.int32, (rows, states), 0)
    col = lax.broadcasted_iota(jnp.int32, (rows, states), 1)
    first = pairs * wide
    wide_group = 2 * (col // wide)
    narrow_group = 2 * ((col - first) // ((states - first) // pairs)) + 1
    return row // group == jnp.where(col < first, wide_group, narrow_group)


def spread_blocks(compact, mask, groups):
    states = mask.shape[1]
    tall = jnp.concatenate([compact] * groups, axis=0)
    zero = jnp.zeros((), tall.dtype)
    return jnp.concatenate(
        [jnp.where(mask, tall[:, part * states : (part + 1) * states], zero) for part in range(2)],
        axis=1,
    )


def prepare(dims, drive_ref, forget_ref, terms_ref, in_ref, rows_ref, push_ref, log_ref):
    pairs, group, wide, states = dims
    groups = 2 * pairs
    span = drive_ref.shape[0] // CHUNKS
    for chunk in range(CHUNKS):
        rows_ref[pl.ds(chunk, span, stride=CHUNKS), :] = drive_ref[
            chunk * span : (chunk + 1) * span, :
        ].astype(f32)
    mask = owners(groups * group, states, pairs, group, wide)
    in_block = spread_blocks(in_ref[...].astype(f32), mask, groups).astype(bf16)
    pushed = jnp.dot(rows_ref[...].astype(bf16), in_block, preferred_element_type=f32)
    coef = terms_ref[3:4, :], terms_ref[4:5, :]
    push_real, push_imag = times((pushed[:, :states], pushed[:, states:]), coef)
    push_ref[:, :states] = push_real
    push_ref[:, states:] = push_imag
    spread = owners(groups, states, pairs, 1, wide).astype(f32)
    log_ref[...] = jnp.dot(
        forget_ref[...], spread, precision=lax.Precision.HIGHEST, preferred_element_type=f32
    )


def scan_chunks(states, terms_ref, push_ref, log_ref, start, keep):
    span = push_ref.shape[0] // CHUNKS
    growth = jnp.broadcast_to(terms_ref[0:1, :], (CHUNKS, states))
    cosine = jnp.broadcast_to(terms_ref[1:2, :], (CHUNKS, states))
    sine = jnp.broadcast_to(terms_ref[2:3, :], (CHUNKS, states))

    def one(place, carried):
        real, imag, total = carried
        rows = pl.ds(pl.multiple_of(place * CHUNKS, CHUNKS), CHUNKS)
        forget = log_ref[rows, :]
        decay = jnp.exp(growth - forget)
        turned_real = real * cosine - imag * sine
        turned_imag = real * sine + imag * cosine
        real = decay * turned_real + push_ref[rows, :states]
        imag = decay * turned_imag + push_ref[rows, states:]
        if keep is not None:
            keep(rows, real, imag)
        return real, imag, total + forget

    zero = jnp.zeros((CHUNKS, states), f32)
    return lax.fori_loop(0, span, one, (*start, zero), unroll=8)


def step_factor(terms_ref, forget, length):
    phase = power_of((terms_ref[1:2, :], terms_ref[2:3, :]), length)
    size = jnp.exp(length * terms_ref[0:1, :] - forget)
    return size * phase[0], size * phase[1]


def alternate_lanes(shape):
    return (lax.broadcasted_iota(jnp.int32, shape, len(shape) - 1) // 32) % 2 == 0


def ends_kernel(dims, drive_ref, forget_ref, terms_ref, in_ref, sent_ref, ends_ref, rows_ref, push_ref, log_ref):
    states = dims[3]
    prepare(dims, drive_ref, forget_ref, terms_ref, in_ref, rows_ref, push_ref, log_ref)
    zero = jnp.zeros((CHUNKS, states), f32)
    real, imag, total = scan_chunks(states, terms_ref, push_ref, log_ref, (zero, zero), None)
    ends_ref[0] = real
    ends_ref[1] = imag
    ends_ref[2] = total
    span = push_ref.shape[0] // CHUNKS
    factor = step_factor(terms_ref, total, span)
    state = real[0:1], imag[0:1]
    for chunk in range(1, CHUNKS):
        at = slice(chunk, chunk + 1)
        turned = times((factor[0][at], factor[1][at]), state)
        state = turned[0] + real[at], turned[1] + imag[at]
    whole = jnp.sum(total, axis=0, keepdims=True)
    for part in range(2):
        for tile in range(3):
            sent_ref[3 * part + tile : 3 * part + tile + 1, :] = state[part][
                :, tile * LANES : (tile + 1) * LANES
            ]
    first, second, third = (whole[:, tile * LANES : (tile + 1) * LANES] for tile in range(3))
    sent_ref[6:7, :] = jnp.where(alternate_lanes((1, LANES)), first, second)
    sent_ref[7:8, :] = third


def active_kernel(
    dims,
    here_ref,
    all_ref,
    ends_ref,
    drive_ref,
    forget_ref,
    terms_ref,
    in_ref,
    out_ref,
    skip_ref,
    gain_ref,
    active_ref,
    rows_ref,
    push_ref,
    log_ref,
    state_ref,
):
    pairs, group, wide, states = dims
    prepare(dims, drive_ref, forget_ref, terms_ref, in_ref, rows_ref, push_ref, log_ref)
    length = push_ref.shape[0]
    span = length // CHUNKS

    growth = terms_ref[0:1, :] * length
    phase = power_of((terms_ref[1:2, :], terms_ref[2:3, :]), length)
    even = alternate_lanes((1, LANES))

    def join(tile, at):
        return jnp.concatenate([tile[at + k : at + k + 1, :] for k in range(3)], axis=1)

    def one(device, state):
        tile = all_ref[device]
        packed = tile[6:7, :]
        first = jnp.where(even, packed, pltpu.roll(packed, 32, 1))
        second = jnp.where(even, pltpu.roll(packed, LANES - 32, 1), packed)
        forget = jnp.concatenate([first, second, tile[7:8, :]], axis=1)
        size = jnp.exp(growth - forget)
        turned = times(phase, state)
        return size * turned[0] + join(tile, 0), size * turned[1] + join(tile, 3)

    none = jnp.zeros((1, states), f32)
    state = lax.fori_loop(0, here_ref[0], one, (none, none))

    factor = step_factor(terms_ref, ends_ref[2], span)
    starts = [state]
    for chunk in range(CHUNKS - 1):
        at = slice(chunk, chunk + 1)
        turned = times((factor[0][at], factor[1][at]), state)
        state = turned[0] + ends_ref[0, at], turned[1] + ends_ref[1, at]
        starts.append(state)
    start = tuple(jnp.concatenate([item[part] for item in starts], axis=0) for part in range(2))

    def keep(rows, real, imag):
        state_ref[rows, :states] = real
        state_ref[rows, states:] = imag

    scan_chunks(states, terms_ref, push_ref, log_ref, start, keep)

    mask = owners(2 * pairs * group, states, pairs, group, wide)
    out_block = spread_blocks(out_ref[...].astype(f32), mask, 2 * pairs).astype(bf16)
    value = state_ref[...]
    high = value.astype(bf16)
    low = (value - high.astype(f32)).astype(bf16)
    over = (((1,), (1,)), ((), ()))
    response = lax.dot_general(high, out_block, over, preferred_element_type=f32)
    response = response + lax.dot_general(low, out_block, over, preferred_element_type=f32)
    response = response + skip_ref[...] * rows_ref[...]
    rows_ref[...] = 0.5 * response * (1.0 + lax.erf(response * 0.7071067811865476))
    for chunk in range(CHUNKS):
        active_ref[chunk * span : (chunk + 1) * span, :] = rows_ref[
            pl.ds(chunk, span, stride=CHUNKS), :
        ].astype(bf16)
    gain, parts = gain_ref[...], []
    for _ in range(3):
        parts.append(gain.astype(bf16))
        gain = gain - parts[-1].astype(f32)
    parts.append(jnp.zeros((GAIN_ROWS - 3, gain.shape[1]), bf16))
    active_ref[length:, :] = jnp.concatenate(parts, axis=0)


def normed_kernel(here_ref, act_ref, gain_ref, same_ref, other_ref, hidden_ref, mlp_ref, normed_ref, own_ref):
    chip, core = here_ref[0] // 2, here_ref[0] % 2
    chips = same_ref.shape[0]
    active = act_ref[...].astype(f32)
    power = jnp.sum(jnp.sum(active * active, axis=0), axis=1, keepdims=True)
    channels = act_ref.shape[0] * act_ref.shape[2]
    scale = lax.rsqrt(power / channels + epsilon)

    def mixed(block):
        gain = jnp.sum(gain_ref[block].astype(f32), axis=0, keepdims=True)
        return (act_ref[block].astype(f32) * scale * gain).astype(bf16)

    total = jnp.zeros(hidden_ref.shape, f32)
    for back in range(chips):
        base = 2 * lax.rem(chip + chips - back, chips)
        total += jnp.dot(mixed(base + core), same_ref[back], preferred_element_type=f32)
        total += jnp.dot(mixed(base + 1 - core), other_ref[back], preferred_element_type=f32)
    carried = (hidden_ref[...].astype(f32) + total).astype(bf16)
    values = carried.astype(f32)
    normed_ref[...] = (
        values * lax.rsqrt(jnp.mean(values * values, axis=1, keepdims=True) + epsilon) * mlp_ref[...]
    ).astype(bf16)

    @pl.when(pl.program_id(0) == here_ref[0])
    def _():
        own_ref[...] = carried


def mixer_kernel(here_ref, normed_ref, weight_ref, own_ref, other_ref, up_ref, down_ref, up_sem, down_sem):
    blocks, parts = up_sem.shape[0], up_ref.shape[0] // up_sem.shape[0]
    width = up_ref.shape[1]

    def copies(block):
        at = pl.ds(block * parts, parts)
        return (
            pltpu.make_async_copy(weight_ref.at[at, pl.ds(0, width), :], up_ref.at[at], up_sem.at[block]),
            pltpu.make_async_copy(
                weight_ref.at[at, pl.ds(width, width), :], down_ref.at[at], down_sem.at[block]
            ),
        )

    for which in range(2):
        for block in range(blocks):
            copies(block)[which].start()
    rows, hidden = normed_ref.shape[0], up_ref.shape[2]
    depth = parts * width
    total = jnp.zeros((rows, hidden), f32)
    for block in range(blocks):
        copies(block)[0].wait()
        piece = up_ref[block * parts : (block + 1) * parts].reshape(depth, hidden)
        total += jnp.dot(
            normed_ref[:, block * depth : (block + 1) * depth], piece, preferred_element_type=f32
        )
    squared = jnp.square(jnp.maximum(total, 0.0)).astype(bf16)
    core = here_ref[0] % 2
    share = own_ref.shape[1]
    for block in range(blocks):
        copies(block)[1].wait()
        piece = down_ref[block * parts : (block + 1) * parts].reshape(depth, hidden)
        value = lax.dot_general(
            squared, piece, (((1,), (1,)), ((), ())), preferred_element_type=f32
        ).astype(bf16)
        value = value.reshape(own_ref.shape[0], 2, share, depth)
        at = slice(block * depth, (block + 1) * depth)
        own_ref[:, :, at] = jnp.where(core == 0, value[:, 0], value[:, 1])
        other_ref[:, :, at] = jnp.where(core == 0, value[:, 1], value[:, 0])


def local(
    hidden_in,
    drive,
    wide_poles,
    narrow_poles,
    log_step,
    forget,
    wide_input,
    narrow_input,
    wide_output,
    narrow_output,
    skip,
    mix_gain,
    out_weight,
    mlp_gain,
    up_weight,
    down_weight,
):
    rows, model = hidden_in.shape
    count = lax.axis_size("tp")
    chips, share = count // 2, rows // count
    pairs, wide = wide_poles.shape[1:]
    group = wide_input.shape[3]
    states = pairs * (wide + narrow_poles.shape[2])
    dims = (pairs, group, wide, states)
    here = lax.axis_index("tp").reshape(1)
    same_core = [[2 * chip + core for chip in range(chips)] for core in range(2)]

    weights = lax.all_gather(jnp.concatenate([up_weight, down_weight], axis=0), "sp", axis=0)

    def from_chip(value, back):
        return lax.ppermute(value, "tp", [(i, (i + 2 * back) % count) for i in range(count)])

    def swap(value):
        return lax.ppermute(value, "tp", [(i, i ^ 1) for i in range(count)])

    out_same = jnp.stack([out_weight] + [from_chip(out_weight, back) for back in range(1, chips)])
    out_other = swap(out_same)

    terms = jnp.concatenate(
        [discretize(wide_poles, log_step[:, 0]), discretize(narrow_poles, log_step[:, 1])], axis=1
    )
    forget_rows = jnp.transpose(
        forget.reshape(2 * pairs, CHUNKS, rows // CHUNKS), (2, 1, 0)
    ).reshape(rows, 2 * pairs)

    def compact(first, second, order):
        first, second = (
            jnp.transpose(item, order).reshape(group, 2, -1) for item in (first, second)
        )
        return jnp.concatenate([first, second], axis=2).reshape(group, 2 * states)

    in_compact = compact(wide_input, narrow_input, (3, 0, 1, 2))
    out_compact = compact(
        wide_output * jnp.array([1, -1], bf16)[:, None, None, None],
        narrow_output * jnp.array([1, -1], bf16)[:, None, None, None],
        (2, 0, 1, 3),
    )
    channels = drive.shape[1]
    scratch = [
        pltpu.VMEM((rows, channels), f32),
        pltpu.VMEM((rows, 2 * states), f32),
        pltpu.VMEM((rows, states), f32),
    ]
    sent, ends = pl.pallas_call(
        functools.partial(ends_kernel, dims),
        out_shape=[
            jax.ShapeDtypeStruct((8, LANES), f32),
            jax.ShapeDtypeStruct((3, CHUNKS, states), f32),
        ],
        in_specs=[WHOLE] * 4,
        out_specs=[WHOLE] * 2,
        scratch_shapes=scratch,
        name="ends",
    )(drive, forget_rows, terms, in_compact)
    everyone = copy_for_each(sent[None], "sp").reshape(-1, *sent.shape)
    active = pl.pallas_call(
        functools.partial(active_kernel, dims),
        out_shape=jax.ShapeDtypeStruct((rows + GAIN_ROWS, channels), bf16),
        in_specs=[SCALARS] + [WHOLE] * 9,
        out_specs=WHOLE,
        scratch_shapes=scratch + [pltpu.VMEM((rows, 2 * states), f32)],
        name="active",
    )(
        lax.axis_index("sp").reshape(1),
        everyone,
        ends,
        drive,
        forget_rows,
        terms,
        in_compact,
        out_compact,
        skip[None],
        mix_gain[None],
    )
    gathered = lax.all_gather(active, "tp", axis=0)
    normed, own_rows = pl.pallas_call(
        normed_kernel,
        grid=(count,),
        out_shape=[
            jax.ShapeDtypeStruct((rows, model), bf16),
            jax.ShapeDtypeStruct((share, model), bf16),
        ],
        in_specs=[
            SCALARS,
            pl.BlockSpec((count, share, channels), lambda i: (0, i, 0)),
            pl.BlockSpec((count, GAIN_ROWS, channels), lambda i: (0, rows // GAIN_ROWS, 0)),
            pl.BlockSpec(out_same.shape, lambda i: (0, 0, 0)),
            pl.BlockSpec(out_same.shape, lambda i: (0, 0, 0)),
            pl.BlockSpec((share, model), lambda i: (i, 0)),
            pl.BlockSpec((1, model), lambda i: (0, 0)),
        ],
        out_specs=[
            pl.BlockSpec((share, model), lambda i: (i, 0)),
            pl.BlockSpec((share, model), lambda i: (0, 0)),
        ],
        name="normed",
    )(here, gathered, gathered, out_same, out_other, hidden_in, mlp_gain[None])
    devices, width, hidden = weights.shape[0], up_weight.shape[0], up_weight.shape[1]
    own_part, other_part = pl.pallas_call(
        mixer_kernel,
        out_shape=[jax.ShapeDtypeStruct((chips, share, model), bf16)] * 2,
        in_specs=[SCALARS, WHOLE, pl.BlockSpec(memory_space=pl.ANY)],
        out_specs=[WHOLE] * 2,
        scratch_shapes=[
            pltpu.VMEM((devices, width, hidden), bf16),
            pltpu.VMEM((devices, width, hidden), bf16),
            pltpu.SemaphoreType.DMA((8,)),
            pltpu.SemaphoreType.DMA((8,)),
        ],
        name="mixer",
    )(here, normed, weights)
    chip_part = (own_part.astype(f32) + swap(other_part).astype(f32)).astype(bf16)
    pieces = lax.all_to_all(chip_part, "tp", 0, 0, tiled=True, axis_index_groups=same_core)
    total = jnp.sum(pieces.astype(f32), axis=0)
    finished = (own_rows.astype(f32) + total).astype(bf16)
    mine = copy_for_each(finished[None], "tp", same_core)
    theirs = swap(mine)
    first = here[0] % 2 == 0
    return jnp.stack(
        [jnp.where(first, mine, theirs), jnp.where(first, theirs, mine)], axis=1
    ).reshape(rows, model)


def solution(mesh):
    return jax.shard_map(
        local,
        mesh=mesh,
        in_specs=(
            P("sp", None),
            P("sp", "tp"),
            P(None, "tp", None),
            P(None, "tp", None),
            P("tp", None),
            P("tp", None, "sp"),
            P(None, "tp", None, None),
            P(None, "tp", None, None),
            P(None, "tp", None, None),
            P(None, "tp", None, None),
            P("tp"),
            P("tp"),
            P("tp", None),
            P(),
            P("sp", "tp"),
            P("sp", "tp"),
        ),
        out_specs=P("sp", None),
        check_vma=False,
    )
```

time: 438 us -> 180 us (0.41); the launches traced: 431 us -> 179 us
  local copies, waits for them, and re-layouts: 221 us -> 6.89 us
  blocking collectives: 85 us -> 45.8 us
  other arithmetic: 42.6 us -> 6.92 us
  Pallas kernels: 0 us -> 28.6 us
  starting transfers between devices: 21.6 us -> 39.7 us
  matrix products: 13.5 us -> 0 us
  waiting for transfers between devices: 29.7 us -> 37.5 us
    slice x306 -> x0, local copies, waits for them, and re-layouts: 196 us -> none  [the longest x224 146 us: kind_states(): lax.associative_scan(combine, (spike_magnitude * jnp.cos(angle)[None], sp...]
    all_to_all x3 -> x1, blocking collectives: 59.9 us -> 13 us  [copy_for_each(): lax.all_to_all(jnp.broadcast_to(value[None], (count, *value.shape)), axis...]
    pallas_call x0 -> x4, Pallas kernels: none -> 28.6 us  [the longest x1 11.2 us: local(): pl.pallas_call(normed_kernel, grid=(count,), out_shape=[jax.ShapeDtypeStr...]
    ppermute x0 -> x6, starting transfers between devices: none -> 23.3 us  [the longest x3 11.9 us: swap(): return lax.ppermute(value, 'tp', [(i, i ^ 1) for i in range(count)])]
    all_to_all x1 -> x0, waiting for transfers between devices: 20.6 us -> none  [sum_at_owner(): pieces = lax.all_to_all(split_up(value, dim, count), axis, 0, 0, tiled=True)]
    ppermute x0 -> x6, waiting for transfers between devices: none -> 20.4 us  [the longest x3 16.4 us: from_chip(): lax.ppermute(value, 'tp', [(i, (i + 2 * back) % count) for i in range(cou...]
    all_gather x0 -> x1, blocking collectives: none -> 17.6 us  [local(): gathered = lax.all_gather(active, 'tp', axis=0)]
    add x107 -> x0, other arithmetic: 15.4 us -> none  [the longest x24 7.59 us: combine(): later[0] * earlier[3] + later[1] * earlier[2] + later[3]]
  transfers between devices with their start and end apart: 4 -> 8, of which waited for: 2 -> 5; matrix products, arithmetic and copies ran while one was open for 61% -> 5% of each run, Pallas kernels for 0% -> 10%
where the time goes in v1:
time: 180 us; the launch traced here: 179 us
  blocking collectives  45.8 us (25%)
  starting transfers between devices  39.7 us (22%)
  waiting for transfers between devices  37.5 us (21%)
  Pallas kernels  28.6 us (16%)
  between operations  13.6 us (8%)
  other arithmetic  6.92 us (4%)
  local copies, waits for them, and re-layouts  6.89 us (4%)
    all_gather x1, blocking collectives, local(): gathered = lax.all_gather(active, 'tp', axis=0)  17.6 us
    all_to_all x1, starting transfers between devices, copy_for_each(): lax.all_to_all(jnp.broadcast_to(value[None], (count, *value.shape)), axis...  16.5 us
    ppermute x3, waiting for transfers between devices, from_chip(): lax.ppermute(value, 'tp', [(i, (i + 2 * back) % count) for i in range(cou...  16.4 us
    all_to_all x1, blocking collectives, local(): lax.all_to_all(chip_part, 'tp', 0, 0, tiled=True, axis_index_groups=same_...  15.2 us
    all_to_all x1, blocking collectives, copy_for_each(): lax.all_to_all(jnp.broadcast_to(value[None], (count, *value.shape)), axis...  13 us
    all_to_all x1, waiting for transfers between devices, copy_for_each(): lax.all_to_all(jnp.broadcast_to(value[None], (count, *value.shape)), axis...  12.5 us
    ppermute x3, starting transfers between devices, swap(): return lax.ppermute(value, 'tp', [(i, i ^ 1) for i in range(count)])  11.9 us
    ppermute x3, starting transfers between devices, from_chip(): lax.ppermute(value, 'tp', [(i, (i + 2 * back) % count) for i in range(cou...  11.4 us
  transfers between devices with their start and end apart: 8, of which 5 were waited for; matrix products, arithmetic and copies ran while one was open for 5% of the time, Pallas kernels for 10%

profile of v1, /device:TPU:1, one launch (start us, length us, event | category | flops | bytes accessed | tf_op | source)
XLA Modules:
  0.0 179.1 jit_solution(17042748814738211668)
XLA Ops:
  6.5 0.0 all-gather.4.cloned.1.call-start
  6.5 1.5 pad_maximum_fusion.2
  8.1 0.0 all-gather.4.cloned.1.call-update
  8.1 3.9 %collective-permute-start = (bf16[128,2048]{1,0:T(8,128)(2,1)}, bf16[128,2048]{1,0:T(8,128)(2,1)S(1)}, u32[]{:S(2)}, u32[]{:S(2)}) collective-permute-start(bf16[128,2048]{1,0:T(8,128)(2,1)} %param.30), channel_id=1, source_target_pairs={{0,2},{1,3},{2,4},{3,5},{4,6},{5,7},{6,0},{7,1},{8,10},{9,11},{10,... | collective-permute-start | bytes 1572872 | tf_op jit(solution)/shard_map/ppermute | solution.py:337
  12.0 4.4 %collective-permute-start.1 = (bf16[128,2048]{1,0:T(8,128)(2,1)}, bf16[128,2048]{1,0:T(8,128)(2,1)S(1)}, u32[]{:S(2)}, u32[]{:S(2)}) collective-permute-start(bf16[128,2048]{1,0:T(8,128)(2,1)} %param.30), channel_id=1, source_target_pairs={{0,4},{1,5},{2,6},{3,7},{4,0},{5,1},{6,2},{7,3},{8,12},{9,13},{10,... | collective-permute-start | bytes 1572872 | tf_op jit(solution)/shard_map/ppermute | solution.py:337
  16.4 3.1 %collective-permute-start.2 = (bf16[128,2048]{1,0:T(8,128)(2,1)}, bf16[128,2048]{1,0:T(8,128)(2,1)S(1)}, u32[]{:S(2)}, u32[]{:S(2)}) collective-permute-start(bf16[128,2048]{1,0:T(8,128)(2,1)} %param.30), channel_id=1, source_target_pairs={{0,6},{1,7},{2,0},{3,1},{4,2},{5,3},{6,4},{7,5},{8,14},{9,15},{10,... | collective-permute-start | bytes 1572872 | tf_op jit(solution)/shard_map/ppermute | solution.py:337
  19.5 0.7 fusion
  20.2 0.7 fusion.1
  20.9 0.0 collective-permute-done
  20.9 16.4 %collective-permute-done.1 = bf16[128,2048]{1,0:T(8,128)(2,1)S(1)} collective-permute-done((bf16[128,2048]{1,0:T(8,128)(2,1)}, bf16[128,2048]{1,0:T(8,128)(2,1)S(1)}, u32[]{:S(2)}, u32[]{:S(2)}) %collective-permute-start.1) | collective-permute-done | bytes 524320 | tf_op jit(solution)/shard_map/ppermute | solution.py:337
  37.3 0.0 collective-permute-done.2
  37.3 0.0 copy-start.4
  37.3 0.0 copy-start.5
  37.3 0.0 copy-start.8
  37.3 0.0 copy-start.6
  37.3 1.4 pad_maximum_fusion.same_ref
  38.7 4.8 %collective-permute-start.3 = (bf16[4,128,2048]{2,1,0:T(8,128)(2,1)S(1)}, bf16[4,128,2048]{2,1,0:T(8,128)(2,1)}, u32[]{:S(2)}, u32[]{:S(2)}) collective-permute-start(bf16[4,128,2048]{2,1,0:T(8,128)(2,1)S(1)} %pad_maximum_fusion.same_ref), channel_id=1, source_target_pairs={{0,1},{1,0},{2,3},{3,2},{4,5},{5,4},{6,7},{7,6},{8,9},{9,8},{10,11... | collective-permute-start | bytes 6291464 | tf_op jit(solution)/shard_map/ppermute | solution.py:340
  43.5 0.1 squeeze.8
  43.6 0.1 squeeze.9
  43.7 0.1 mul.325
  43.8 0.1 mul.326
  43.9 0.1 squeeze.10
  43.9 0.1 squeeze.11
  44.0 0.1 mul.340
  44.1 0.1 mul.341
  44.2 0.0 copy-done.7
  44.2 0.1 reshape.438
  44.3 0.8 copy.40
  45.1 0.0 copy-done.3
  45.1 0.1 reshape.440
  45.2 0.1 reshape.441
  45.3 0.6 copy.51
  45.9 0.1 subtract_divide_fusion
  46.0 0.1 add_divide_fusion
  46.1 0.1 subtract_divide_fusion.1
  46.2 0.1 add_divide_fusion.1
  46.3 0.6 pad_maximum_fusion.3.terms_ref
  46.9 2.7 %ends.1 = (f32[8,128]{1,0:T(8,128)}, f32[3,8,384]{2,1,0:T(8,128)}) custom-call(bf16[384,128]{1,0:T(8,128)(2,1)} %drive_ref.3, f32[384,8]{1,0:T(8,128)} %bitcast.53, f32[5,384]{1,0:T(8,128)} %pad_maximum_fusion.3.terms_ref, bf16[16,768]{1,0:T(8,128)(2,1)} %bitcast.60), custom_call_target="tpu_custom_call" | custom-call | tf_op jit(solution)/shard_map/ends/pallas_call | solution.py:370
  49.6 1.4 broadcast_in_dim.10
  51.0 16.5 %all-to-all-start = ((f32[64,1,8,128]{3,2,1,0:T(8,128)}), f32[64,1,8,128]{3,2,1,0:T(8,128)S(1)}, u32[]{:S(2)}, u32[]{:S(2)}) async-start(f32[64,1,8,128]{3,2,1,0:T(8,128)} %broadcast_in_dim.10), calls=%async_computation | async-start | bytes 524288 | tf_op jit(solution)/shard_map/all_to_all | solution.py:21
  67.5 0.1 multiply_bitcast_fusion.1
  67.6 0.1 reshape.444
  67.7 0.1 multiply_bitcast_fusion
  67.8 0.1 reshape.445
  67.9 0.6 copy.52
  68.5 12.5 %all-to-all-done = f32[64,1,8,128]{3,2,1,0:T(8,128)S(1)} async-done(((f32[64,1,8,128]{3,2,1,0:T(8,128)}), f32[64,1,8,128]{3,2,1,0:T(8,128)S(1)}, u32[]{:S(2)}, u32[]{:S(2)}) %all-to-all-start) | async-done | bytes 262176 | tf_op jit(solution)/shard_map/all_to_all | solution.py:21
  81.1 0.7 copy-done.1
  81.8 3.7 %active.1 = bf16[400,128]{1,0:T(8,128)(2,1)} custom-call(s32[1]{0:T(128)} %bitcast.1.here_ref, f32[64,8,128]{2,1,0:T(8,128)} %bitcast.55, f32[3,8,384]{2,1,0:T(8,128)} %get-tuple-element.12.ends_ref, bf16[384,128]{1,0:T(8,128)(2,1)} %drive_ref.3, f32[384,8]{1,0:T(8,128)} %bitcast.54, f32[5,384]{1,0:T(8,128)} %pad_maximum_fusion.3.terms_ref, ...), custom_call_target="tpu_custom_call" | custom-call | tf_op jit(solution)/shard_map/active/pallas_call | solution.py:382
  85.4 17.6 %all-gather = bf16[3200,128]{1,0:T(8,128)(2,1)} all-gather(bf16[400,128]{1,0:T(8,128)(2,1)} %active.1), channel_id=2, replica_groups=mesh['sp'=64,'tp'=8] {'tp'}, dimensions={0}, use_global_device_ids=true | all-gather | bytes 921600 | tf_op jit(solution)/shard_map/all_gather | solution.py:401
  103.0 0.0 collective-permute-done.3.other_ref
  103.0 11.2 %normed.1 = (bf16[384,2048]{1,0:T(8,128)(2,1)}, bf16[48,2048]{1,0:T(8,128)(2,1)}) custom-call(s32[1]{0:T(128)} %bitcast.here_ref, bf16[8,400,128]{2,1,0:T(8,128)(2,1)} %bitcast.50, bf16[8,400,128]{2,1,0:T(8,128)(2,1)} %bitcast.51, bf16[4,128,2048]{2,1,0:T(8,128)(2,1)} %copy-done, bf16[4,128,2048]{2,1,0:T(8,128)(2,1)} %collective-permute-done.3.other_ref, ...), custom_call_target="tpu_custom_call" | custom-call | tf_op jit(solution)/shard_map/normed/pallas_call | solution.py:402
  114.2 4.6 %all-gather.4.cloned.1.call-done = bf16[4096,1024]{1,0:T(8,128)(2,1)} async-done(((bf16[64,1024]{1,0:T(8,128)(2,1)}), bf16[4096,1024]{1,0:T(8,128)(2,1)}) %all-gather.4.cloned.1.call-update) | async-done | bytes 8388624 | tf_op jit(solution)/shard_map/all_gather | solution.py:334
  118.8 11.1 %mixer.1 = (bf16[4,48,2048]{2,1,0:T(8,128)(2,1)}, bf16[4,48,2048]{2,1,0:T(8,128)(2,1)}) custom-call(s32[1]{0:T(128)} %bitcast.here_ref, bf16[384,2048]{1,0:T(8,128)(2,1)} %get-tuple-element.14.normed_ref, bf16[64,64,1024]{2,1,0:T(8,128)(2,1)} %bitcast.49), custom_call_target="tpu_custom_call" | custom-call | tf_op jit(solution)/shard_map/mixer/pallas_call | solution.py:425
  129.9 2.5 %collective-permute-start.4 = (bf16[4,48,2048]{2,1,0:T(8,128)(2,1)}, bf16[4,48,2048]{2,1,0:T(8,128)(2,1)S(1)}, u32[]{:S(2)}, u32[]{:S(2)}) collective-permute-start(bf16[4,48,2048]{2,1,0:T(8,128)(2,1)} %get-tuple-element.16), channel_id=1, source_target_pairs={{0,1},{1,0},{2,3},{3,2},{4,5},{5,4},{6,7},{7,6},{8,9},{9,8},{10,11... | collective-permute-start | bytes 2359304 | tf_op jit(solution)/shard_map/ppermute | solution.py:340
  132.4 2.1 %collective-permute-done.4 = bf16[4,48,2048]{2,1,0:T(8,128)(2,1)S(1)} collective-permute-done((bf16[4,48,2048]{2,1,0:T(8,128)(2,1)}, bf16[4,48,2048]{2,1,0:T(8,128)(2,1)S(1)}, u32[]{:S(2)}, u32[]{:S(2)}) %collective-permute-start.4) | collective-permute-done | bytes 786464 | tf_op jit(solution)/shard_map/ppermute | solution.py:340
  134.5 1.4 add_convert_fusion
  135.9 15.2 %all_to_all.15 = bf16[4,48,2048]{2,1,0:T(8,128)(2,1)S(1)} all-to-all(bf16[4,48,2048]{2,1,0:T(8,128)(2,1)S(1)} %add_convert_fusion), channel_id=1, replica_groups={{0,2,4,6},{1,3,5,7},{8,10,12,14},{9,11,13,15},{16,18,20,22},{17,19,21,2..., dimensions={0} | all-to-all | bytes 1572864 | tf_op jit(solution)/shard_map/all_to_all | solution.py:439
  151.2 0.1 convert_reduce_fusion
  151.3 0.1 broadcast_in_dim.27
  151.4 13.0 %all_to_all.16 = bf16[4,1,48,2048]{3,2,1,0:T(8,128)(2,1)S(1)} all-to-all(bf16[4,1,48,2048]{3,2,1,0:T(8,128)(2,1)S(1)} %broadcast_in_dim.27), channel_id=1, replica_groups={{0,2,4,6},{1,3,5,7},{8,10,12,14},{9,11,13,15},{16,18,20,22},{17,19,21,2..., dimensions={0} | all-to-all | bytes 1572864 | tf_op jit(solution)/shard_map/all_to_all | solution.py:21
  164.4 4.6 %collective-permute-start.5 = (bf16[4,1,48,2048]{3,2,0,1:T(8,128)(2,1)S(1)}, bf16[4,1,48,2048]{3,2,0,1:T(8,128)(2,1)S(1)}, u32[]{:S(2)}, u32[]{:S(2)}) collective-permute-start(bf16[4,1,48,2048]{3,2,0,1:T(8,128)(2,1)S(1)} %bitcast.52), channel_id=1, source_target_pairs={{0,1},{1,0},{2,3},{3,2},{4,5},{5,4},{6,7},{7,6},{8,9},{9,8},{10,11... | collective-permute-start | bytes 2359304 | tf_op jit(solution)/shard_map/ppermute | solution.py:340
  169.0 1.9 %collective-permute-done.5 = bf16[4,1,48,2048]{3,2,0,1:T(8,128)(2,1)S(1)} collective-permute-done((bf16[4,1,48,2048]{3,2,0,1:T(8,128)(2,1)S(1)}, bf16[4,1,48,2048]{3,2,0,1:T(8,128)(2,1)S(1)}, u32[]{:S(2)}, u32[]{:S(2)}) %collective-permute-start.5) | collective-permute-done | bytes 786464 | tf_op jit(solution)/shard_map/ppermute | solution.py:340
  170.9 0.1 select_bitcast_fusion.1
  171.0 1.3 pad_maximum_fusion.1
  (23 shorter events, 0.2 us)
Async XLA Ops:
  6.5 112.3 %all-gather.4.cloned.1.call-start = ((), (), s32[]{:S(2)}) async-start(), calls=%async_computation.3 | async-start | bytes 8519680 | tf_op jit(solution)/shard_map/all_gather | solution.py:334
  8.1 12.8 %collective-permute-start = (bf16[128,2048]{1,0:T(8,128)(2,1)}, bf16[128,2048]{1,0:T(8,128)(2,1)S(1)}, u32[]{:S(2)}, u32[]{:S(2)}) collective-permute-start(bf16[128,2048]{1,0:T(8,128)(2,1)} %param.30), channel_id=1, source_target_pairs={{0,2},{1,3},{2,4},{3,5},{4,6},{5,7},{6,0},{7,1},{8,10},{9,11},{10,... | collective-permute-start | bytes 1572872 | tf_op jit(solution)/shard_map/ppermute | solution.py:337
  12.0 25.2 %collective-permute-start.1 = (bf16[128,2048]{1,0:T(8,128)(2,1)}, bf16[128,2048]{1,0:T(8,128)(2,1)S(1)}, u32[]{:S(2)}, u32[]{:S(2)}) collective-permute-start(bf16[128,2048]{1,0:T(8,128)(2,1)} %param.30), channel_id=1, source_target_pairs={{0,4},{1,5},{2,6},{3,7},{4,0},{5,1},{6,2},{7,3},{8,12},{9,13},{10,... | collective-permute-start | bytes 1572872 | tf_op jit(solution)/shard_map/ppermute | solution.py:337
  16.4 20.9 %collective-permute-start.2 = (bf16[128,2048]{1,0:T(8,128)(2,1)}, bf16[128,2048]{1,0:T(8,128)(2,1)S(1)}, u32[]{:S(2)}, u32[]{:S(2)}) collective-permute-start(bf16[128,2048]{1,0:T(8,128)(2,1)} %param.30), channel_id=1, source_target_pairs={{0,6},{1,7},{2,0},{3,1},{4,2},{5,3},{6,4},{7,5},{8,14},{9,15},{10,... | collective-permute-start | bytes 1572872 | tf_op jit(solution)/shard_map/ppermute | solution.py:337
  37.3 6.3 %copy-start.9 = (f32[4,2]{0,1:T(2,128)S(1)}, f32[4,2]{0,1:T(2,128)}, u32[]{:S(2)}) copy-start(f32[4,2]{0,1:T(2,128)} %param.22) | copy-start | bytes 100
  37.3 6.9 %copy-start.7 = (f32[4,2,384]{2,1,0:T(2,128)S(1)}, f32[4,2,384]{2,1,0:T(2,128)}, u32[]{:S(2)}) copy-start(f32[4,2,384]{2,1,0:T(2,128)} %param.23) | copy-start | bytes 36868
  37.3 7.8 %copy-start.3 = (bf16[2,4,64,16]{2,3,1,0:T(8,128)(2,1)S(1)}, bf16[2,4,64,16]{2,3,1,0:T(8,128)(2,1)}, u32[]{:S(2)}) copy-start(bf16[2,4,64,16]{2,3,1,0:T(8,128)(2,1)} %param.24) | copy-start | bytes 49156
  37.3 7.9 %copy-start.4 = (bf16[2,4,32,16]{2,3,1,0:T(8,128)(2,1)S(1)}, bf16[2,4,32,16]{2,3,1,0:T(8,128)(2,1)}, u32[]{:S(2)}) copy-start(bf16[2,4,32,16]{2,3,1,0:T(8,128)(2,1)} %param.25) | copy-start | bytes 24580
  37.3 30.2 %copy-start.5 = (bf16[2,4,16,64]{3,2,1,0:T(8,128)(2,1)S(1)}, bf16[2,4,16,64]{3,2,1,0:T(8,128)(2,1)}, u32[]{:S(2)}) copy-start(bf16[2,4,16,64]{3,2,1,0:T(8,128)(2,1)} %param.26) | copy-start | bytes 49156
  37.3 30.2 %copy-start.8 = (bf16[2]{0:T(256)(128)(2,1)S(1)}, bf16[2]{0:T(256)(128)(2,1)}, u32[]{:S(2)}) copy-start(bf16[2]{0:T(256)(128)(2,1)} %constant.33.clone) | copy-start | bytes 16
  37.3 30.4 %copy-start.6 = (bf16[2,4,16,32]{3,2,1,0:T(8,128)(2,1)S(1)}, bf16[2,4,16,32]{3,2,1,0:T(8,128)(2,1)}, u32[]{:S(2)}) copy-start(bf16[2,4,16,32]{3,2,1,0:T(8,128)(2,1)} %param.27) | copy-start | bytes 24580
  38.7 64.3 %copy-start = (bf16[4,128,2048]{2,1,0:T(8,128)(2,1)}, bf16[4,128,2048]{2,1,0:T(8,128)(2,1)S(1)}, u32[]{:S(2)}) copy-start(bf16[4,128,2048]{2,1,0:T(8,128)(2,1)S(1)} %pad_maximum_fusion.same_ref) | copy-start | bytes 6291460
  38.7 64.3 %collective-permute-start.3 = (bf16[4,128,2048]{2,1,0:T(8,128)(2,1)S(1)}, bf16[4,128,2048]{2,1,0:T(8,128)(2,1)}, u32[]{:S(2)}, u32[]{:S(2)}) collective-permute-start(bf16[4,128,2048]{2,1,0:T(8,128)(2,1)S(1)} %pad_maximum_fusion.same_ref), channel_id=1, source_target_pairs={{0,1},{1,0},{2,3},{3,2},{4,5},{5,4},{6,7},{7,6},{8,9},{9,8},{10,11... | collective-permute-start | bytes 6291464 | tf_op jit(solution)/shard_map/ppermute | solution.py:340
  51.0 30.0 %all-to-all-start = ((f32[64,1,8,128]{3,2,1,0:T(8,128)}), f32[64,1,8,128]{3,2,1,0:T(8,128)S(1)}, u32[]{:S(2)}, u32[]{:S(2)}) async-start(f32[64,1,8,128]{3,2,1,0:T(8,128)} %broadcast_in_dim.10), calls=%async_computation | async-start | bytes 524288 | tf_op jit(solution)/shard_map/all_to_all | solution.py:21
  81.1 0.7 copy-start.1
  129.9 4.6 %collective-permute-start.4 = (bf16[4,48,2048]{2,1,0:T(8,128)(2,1)}, bf16[4,48,2048]{2,1,0:T(8,128)(2,1)S(1)}, u32[]{:S(2)}, u32[]{:S(2)}) collective-permute-start(bf16[4,48,2048]{2,1,0:T(8,128)(2,1)} %get-tuple-element.16), channel_id=1, source_target_pairs={{0,1},{1,0},{2,3},{3,2},{4,5},{5,4},{6,7},{7,6},{8,9},{9,8},{10,11... | collective-permute-start | bytes 2359304 | tf_op jit(solution)/shard_map/ppermute | solution.py:340
  134.5 16.8 %copy-start.2 = (bf16[48,2048]{1,0:T(8,128)(2,1)S(1)}, bf16[48,2048]{1,0:T(8,128)(2,1)}, u32[]{:S(2)}) copy-start(bf16[48,2048]{1,0:T(8,128)(2,1)} %get-tuple-element.13) | copy-start | bytes 589828
  164.4 6.5 %collective-permute-start.5 = (bf16[4,1,48,2048]{3,2,0,1:T(8,128)(2,1)S(1)}, bf16[4,1,48,2048]{3,2,0,1:T(8,128)(2,1)S(1)}, u32[]{:S(2)}, u32[]{:S(2)}) collective-permute-start(bf16[4,1,48,2048]{3,2,0,1:T(8,128)(2,1)S(1)} %bitcast.52), channel_id=1, source_target_pairs={{0,1},{1,0},{2,3},{3,2},{4,5},{5,4},{6,7},{7,6},{8,9},{9,8},{10,11... | collective-permute-start | bytes 2359304 | tf_op jit(solution)/shard_map/ppermute | solution.py:340
Sparse Core Ops, SparseCore 0:
  10.4 108.3 all-gather.3
